TPU v7x, 32 devices: a whole 2x2x4 slice. The times are simulated.
32 devices in a mesh: sp: 8 (over z, y), tp: 4 (over x, core).
Axes of the slice: x: 2, y: 2, z: 4, core: 2. Of those that a mesh axis runs over, the one named last changes fastest.
Arguments:
- stream: bfloat16 [2048, 2048], P('sp'), may hold values from -3 to 3
- first_group_queries: bfloat16 [2048, 512], P('sp', 'tp'), may hold values from -6 to 6
- first_group_keys: bfloat16 [2048, 512], P('sp', 'tp'), may hold values from -6 to 6
- first_group_values: bfloat16 [2048, 1024], P('sp', 'tp'), may hold values from -5.5 to 5.5
- first_gate_logits: bfloat16 [2048, 1024], P('sp', 'tp'), may hold values from -6 to 6
- first_decay_logits: bfloat16 [2048, 512], P('sp', 'tp'), may hold values from -4.75 to 14.5
- second_group_queries: bfloat16 [2048, 1024], P('sp', 'tp'), may hold values from -6 to 6
- second_group_keys: bfloat16 [2048, 1024], P('sp', 'tp'), may hold values from -6 to 6
- second_group_values: bfloat16 [2048, 1024], P('sp', 'tp'), may hold values from -5.5 to 5.5
- second_gate_logits: bfloat16 [2048, 1024], P('sp', 'tp'), may hold values from -6 to 6
- second_decay_logits: bfloat16 [2048, 1024], P('sp', 'tp'), may hold values from -4.75 to 14.5
- position_log_decay: float32 [2048], P('sp'), may hold values from -0.6932 to 0, as said below
- per_head_norm_gain: float32 [128], replicated, may hold values from 0.1 to 1.9
- first_output_weight: bfloat16 [1024, 2048], P('tp'), may hold values from -0.125 to 0.125
- second_output_weight: bfloat16 [1024, 2048], P('tp'), may hold values from -0.125 to 0.125
- feedforward_norm_gain: float32 [2048], replicated, may hold values from 0.1 to 1.9
- gate_weight: bfloat16 [2048, 5632], P('sp', 'tp'), may hold values from -0.125 to 0.125
- up_weight: bfloat16 [2048, 5632], P('sp', 'tp'), may hold values from -0.125 to 0.125
- down_weight: bfloat16 [5632, 2048], P('tp', 'sp'), may hold values from -0.078125 to 0.078125
Outputs:
- refined: bfloat16 [2048, 2048], P(('sp', 'tp'))
Inputs may be any that keep to these rules, and one draw needn't show every extreme that they name: `position_log_decay`: most positions carry 0.
All inputs are finite; a program needn't handle non-finite values.
Results may differ from a plain program's by a relative error of at most 0.018.
Values may be sent and summed in bfloat16 or wider, within the bound.
A program may use at most 64 MiB of HBM per device.

v0:
```python
import jax
import jax.numpy as jnp
from jax import lax
from jax.sharding import PartitionSpec as P

KEY_SIZE_FIRST = 64
KEY_SIZE_SECOND = 128
DV = 128
BLK = 64
decay_softness = 16.0
norm_eps = 1e-06
highest = lax.Precision.HIGHEST


def channel_log_decays(decay_logits, position_log_decay, key_channels):
    channel_log_decay = (
        jax.nn.log_sigmoid(decay_logits.astype(jnp.float32)) / decay_softness
        + position_log_decay[:, None]
    )
    return channel_log_decay.reshape(decay_logits.shape[0], -1, key_channels)


def one_way(query_matrix, key_matrix, value_matrix, channel_log_decay, start_state):
    length, heads, key_channels = query_matrix.shape
    value_width = value_matrix.shape[-1]
    block_count = length // BLK

    def blocks(member):
        return member.reshape(block_count, BLK, heads, member.shape[-1]).transpose(0, 2, 1, 3)

    query_blocks = blocks(query_matrix)
    key_blocks = blocks(key_matrix)
    value_blocks = blocks(value_matrix)
    running = jnp.cumsum(blocks(channel_log_decay), axis=2)
    block_last = running[:, :, -1:, :]
    query_in = query_blocks * jnp.exp(running)
    key_in = key_blocks * jnp.exp(-running)
    key_end = key_blocks * jnp.exp(block_last - running)
    places = jnp.arange(BLK, dtype=jnp.int32)
    lower = places[:, None] >= places[None, :]
    scores = jnp.where(
        lower, jnp.einsum("nhid,nhjd->nhij", query_in, key_in, precision=highest), 0.0
    )
    local_out = jnp.einsum("nhij,nhjv->nhiv", scores, value_blocks, precision=highest)

    def advance(states, inputs):
        query_part, key_part, value_part, last_part = inputs
        emitted = jnp.einsum("hid,hdv->hiv", query_part, states, precision=highest)
        states = states * jnp.exp(last_part)[:, 0, :, None] + jnp.einsum(
            "hjd,hjv->hdv", key_part, value_part, precision=highest
        )
        return (states, emitted)

    _, carried = lax.scan(advance, start_state, (query_in, key_end, value_blocks, block_last))
    return (local_out + carried).transpose(0, 2, 1, 3).reshape(length, heads, value_width)


def prepare_inputs(
    query_matrix, key_matrix, value_matrix, decay_logits, position_log_decay, key_channels
):
    length = query_matrix.shape[0]
    channel_log_decay = channel_log_decays(decay_logits, position_log_decay, key_channels)
    query_f = query_matrix.astype(jnp.float32).reshape(length, -1, key_channels)
    key_f = key_matrix.astype(jnp.float32).reshape(length, -1, key_channels)
    value_f = value_matrix.astype(jnp.float32).reshape(length, -1, DV)
    return (query_f, key_f, value_f, channel_log_decay)


def flipped(members):
    return tuple((jnp.flip(member, axis=0) for member in members))


def end_state(members):
    key_f, value_f, channel_log_decay = (members[1], members[2], members[3])
    totals = jnp.sum(channel_log_decay, axis=0)
    running = jnp.cumsum(channel_log_decay, axis=0)
    weighted = key_f * jnp.exp(totals[None] - running)
    states = jnp.einsum("thd,thv->hdv", weighted, value_f, precision=highest)
    return (totals, states)


def finish(forward, backward, gate_values, per_head_norm_gain):
    both = forward + backward
    scale = lax.rsqrt(jnp.mean(both * both, axis=-1, keepdims=True) + norm_eps)
    gated = (
        both
        * scale
        * per_head_norm_gain
        * jax.nn.silu(gate_values.astype(jnp.float32).reshape(both.shape))
    )
    return gated.reshape(both.shape[0], -1).astype(jnp.bfloat16)


def rms_rows(rows, feedforward_norm_gain):
    scale = lax.rsqrt(jnp.mean(rows * rows, axis=-1, keepdims=True) + norm_eps)
    return (rows * scale * feedforward_norm_gain).astype(jnp.bfloat16)


def per_device(
    stream,
    first_group_queries,
    first_group_keys,
    first_group_values,
    first_gate_logits,
    first_decay_logits,
    second_group_queries,
    second_group_keys,
    second_group_values,
    second_gate_logits,
    second_decay_logits,
    position_log_decay,
    per_head_norm_gain,
    first_output_weight,
    second_output_weight,
    feedforward_norm_gain,
    gate_weight,
    up_weight,
    down_weight,
):
    tok_rows = stream.shape[0]
    first_group = prepare_inputs(
        first_group_queries,
        first_group_keys,
        first_group_values,
        first_decay_logits,
        position_log_decay,
        KEY_SIZE_FIRST,
    )
    second_group = prepare_inputs(
        second_group_queries,
        second_group_keys,
        second_group_values,
        second_decay_logits,
        position_log_decay,
        KEY_SIZE_SECOND,
    )
    first_back = flipped(first_group)
    second_back = flipped(second_group)
    ahead_first = end_state(first_group)
    ahead_second = end_state(second_group)
    behind_first = end_state(first_back)
    behind_second = end_state(second_back)
    all_first, all_second = (
        lax.all_gather(ahead_first[0][None], "sp", axis=0, tiled=True),
        lax.all_gather(ahead_second[0][None], "sp", axis=0, tiled=True),
    )
    own_place = lax.axis_index("sp")

    def weights_for(all_logs, count):
        running = jnp.cumsum(all_logs, axis=0)
        own_end = running[own_place]
        own_before = own_end - all_logs[own_place]
        their_before = running - all_logs
        ranks = jnp.arange(count, dtype=jnp.int32)
        lower = (ranks < own_place)[:, None, None]
        higher = (ranks > own_place)[:, None, None]
        ahead = jnp.exp(jnp.where(lower, own_before - running, -jnp.inf))
        behind = jnp.exp(jnp.where(higher, their_before - own_end, -jnp.inf))
        return (ahead, behind)

    empty = (
        jnp.zeros_like(ahead_first[1]),
        jnp.zeros_like(ahead_first[1]),
        jnp.zeros_like(ahead_second[1]),
        jnp.zeros_like(ahead_second[1]),
    )
    pieces = (
        lax.all_gather(ahead_first[1][None].astype(jnp.bfloat16), "sp", axis=0, tiled=True).astype(
            jnp.float32
        ),
        lax.all_gather(behind_first[1][None].astype(jnp.bfloat16), "sp", axis=0, tiled=True).astype(
            jnp.float32
        ),
        lax.all_gather(ahead_second[1][None].astype(jnp.bfloat16), "sp", axis=0, tiled=True).astype(
            jnp.float32
        ),
        lax.all_gather(
            behind_second[1][None].astype(jnp.bfloat16), "sp", axis=0, tiled=True
        ).astype(jnp.float32),
    )
    count = pieces[0].shape[0]
    ahead_a, behind_a = weights_for(all_first, count)
    ahead_b, behind_b = weights_for(all_second, count)
    forward_first = one_way(
        first_group[0],
        first_group[1],
        first_group[2],
        first_group[3],
        empty[0] + jnp.einsum("nhd,nhdv->hdv", ahead_a, pieces[0], precision=highest),
    )
    backward_first = jnp.flip(
        one_way(
            first_back[0],
            first_back[1],
            first_back[2],
            first_back[3],
            empty[1] + jnp.einsum("nhd,nhdv->hdv", behind_a, pieces[1], precision=highest),
        ),
        0,
    )
    forward_second = one_way(
        second_group[0],
        second_group[1],
        second_group[2],
        second_group[3],
        empty[2] + jnp.einsum("nhd,nhdv->hdv", ahead_b, pieces[2], precision=highest),
    )
    backward_second = jnp.flip(
        one_way(
            second_back[0],
            second_back[1],
            second_back[2],
            second_back[3],
            empty[3] + jnp.einsum("nhd,nhdv->hdv", behind_b, pieces[3], precision=highest),
        ),
        0,
    )
    first_group_output = finish(
        forward_first, backward_first, first_gate_logits, per_head_norm_gain
    )
    second_group_output = finish(
        forward_second, backward_second, second_gate_logits, per_head_norm_gain
    )
    part_rows = tok_rows // lax.axis_size("tp")
    row_start = lax.axis_index("tp") * part_rows
    summed = lax.psum(
        (
            jnp.dot(first_group_output, first_output_weight, preferred_element_type=jnp.float32)
            + jnp.dot(second_group_output, second_output_weight, preferred_element_type=jnp.float32)
        ).astype(jnp.bfloat16),
        "tp",
    ).astype(jnp.float32)
    residual = stream.astype(jnp.float32) + summed
    normed_all = rms_rows(residual, feedforward_norm_gain)
    own_residual = lax.dynamic_slice_in_dim(residual, row_start, part_rows, 0)
    pieces = (
        lax.all_gather(gate_weight, "sp", axis=0, tiled=True),
        lax.all_gather(up_weight, "sp", axis=0, tiled=True),
    )
    gate_sum = jnp.dot(normed_all, pieces[0], preferred_element_type=jnp.float32)
    up_sum = jnp.dot(normed_all, pieces[1], preferred_element_type=jnp.float32)
    hidden = (jax.nn.silu(gate_sum) * up_sum).astype(jnp.bfloat16)
    down_whole = lax.all_gather(down_weight, "sp", axis=1, tiled=True)
    down_sum = lax.psum_scatter(
        jnp.dot(hidden, down_whole, preferred_element_type=jnp.float32).astype(jnp.bfloat16),
        "tp",
        scatter_dimension=0,
        tiled=True,
    ).astype(jnp.float32)
    return (own_residual + 0.5 * down_sum).astype(jnp.bfloat16)


def solution(mesh):
    in_specs = (
        P("sp", None),
        P("sp", "tp"),
        P("sp", "tp"),
        P("sp", "tp"),
        P("sp", "tp"),
        P("sp", "tp"),
        P("sp", "tp"),
        P("sp", "tp"),
        P("sp", "tp"),
        P("sp", "tp"),
        P("sp", "tp"),
        P("sp"),
        P(),
        P("tp", None),
        P("tp", None),
        P(),
        P("sp", "tp"),
        P("sp", "tp"),
        P("tp", "sp"),
    )
    out_specs = P(("sp", "tp"), None)
    return jax.shard_map(
        per_device, mesh=mesh, in_specs=in_specs, out_specs=out_specs, check_vma=False
    )
```

profile of v0, /device:TPU:0, one launch (start us, length us, event | category | flops | bytes accessed | tf_op | source)
XLA Modules:
  0.0 579.6 jit_solution(15194093987630395146)
XLA Ops:
  7.4 1.0 copy.247
  8.4 0.9 fusion.78
  10.8 0.9 copy.244
  12.8 0.9 reshape.254
  16.2 1.0 reshape.255
  17.4 1.1 reshape.256
  20.7 22.3 %all_gather.27 = f32[8,2,64]{2,1,0:T(2,128)S(1)} all-gather(f32[1,2,64]{2,1,0:T(2,128)S(1)} %broadcast_in_dim.108), channel_id=1, replica_groups=mesh['sp'=8,'tp'=4] {'sp'}, dimensions={0}, use_global_device_ids=true | all-gather | bytes 4608 | tf_op jit(solution)/shard_map/all_gather | solution.py:144
  43.9 1.2 reduce-window.30
  46.7 32.8 %all-gather.1 = bf16[16,64,128]{2,1,0:T(8,128)(2,1)} all-gather(bf16[2,64,128]{2,1,0:T(8,128)(2,1)S(1)} %convolution_convert_fusion.4), channel_id=3, replica_groups=mesh['sp'=8,'tp'=4] {'sp'}, dimensions={0}, use_global_device_ids=true | all-gather | bytes 294912 | tf_op jit(solution)/shard_map/all_gather | solution.py:171
  80.6 1.6 fusion.71
  83.0 4.6 while.49
  88.2 1.4 fusion.44
  90.5 1.2 reduce-window.26
  92.3 32.8 %all-gather = bf16[16,64,128]{2,1,0:T(8,128)(2,1)} all-gather(bf16[2,64,128]{2,1,0:T(8,128)(2,1)S(1)} %convolution_convert_fusion.3), channel_id=2, replica_groups=mesh['sp'=8,'tp'=4] {'sp'}, dimensions={0}, use_global_device_ids=true | all-gather | bytes 294912 | tf_op jit(solution)/shard_map/all_gather | solution.py:168
  126.8 1.6 fusion.73
  128.4 2.3 while.48
  132.2 16.3 %all_gather.30 = f32[8,2,128]{2,1,0:T(2,128)S(1)} all-gather(f32[1,2,128]{2,1,0:T(2,128)S(1)} %bitcast.424), channel_id=1, replica_groups=mesh['sp'=8,'tp'=4] {'sp'}, dimensions={0}, use_global_device_ids=true | all-gather | bytes 9216 | tf_op jit(solution)/shard_map/all_gather | solution.py:145
  153.3 2.0 rev.40
  155.5 1.4 convolution_convert_fusion.1
  156.9 33.5 %all-gather.3 = bf16[16,128,128]{2,1,0:T(8,128)(2,1)} all-gather(bf16[2,128,128]{2,1,0:T(8,128)(2,1)S(1)} %convolution_convert_fusion.1), channel_id=5, replica_groups=mesh['sp'=8,'tp'=4] {'sp'}, dimensions={0}, use_global_device_ids=true | all-gather | bytes 589824 | tf_op jit(solution)/shard_map/all_gather | solution.py:177
  190.5 1.0 copy.305
  191.7 1.6 rev.37
  193.3 1.1 copy.302
  194.3 1.3 convolution_select_fusion
  196.5 1.2 fusion.46
  198.4 8.6 %while.51 = (s32[]{:T(128)}, f32[2,128,128]{2,1,0:T(8,128)S(1)}, f32[4,2,64,128]{3,2,1,0:T(8,128)}, f32[4,2,1,128]{3,1,2,0:T(2,128)S(1)}, f32[4,2,64,128]{3,2,1,...) while((s32[]{:T(128)}, f32[2,128,128]{2,1,0:T(8,128)S(1)}, ...), condition=%wide.region_26.27_spmd, body=%wide.region_25.26_spmd.sunk | while | flops 50397184 | bytes 660569 | solution.py:54
  199.2 1.2 convolution_add_fusion.16
  201.4 1.2 convolution_add_fusion.16
  203.5 1.2 convolution_add_fusion.16
  205.7 1.2 convolution_add_fusion.16
  206.9 1.3 fusion.42
  210.5 1.1 copy.295
  212.0 33.2 %all-gather.2 = bf16[16,128,128]{2,1,0:T(8,128)(2,1)} all-gather(bf16[2,128,128]{2,1,0:T(8,128)(2,1)S(1)} %convolution_convert_fusion.2), channel_id=4, replica_groups=mesh['sp'=8,'tp'=4] {'sp'}, dimensions={0}, use_global_device_ids=true | all-gather | bytes 589824 | tf_op jit(solution)/shard_map/all_gather | solution.py:174
  245.2 1.1 reshape_reshape.34
  247.7 1.1 reshape_reshape.37
  248.7 2.2 fusion.48
  251.0 2.9 while.50
  254.4 1.0 copy.278
  257.2 1.5 fusion.41
  260.7 33.2 %all-reduce.2.cloned.1.call-done = bf16[256,2048]{1,0:T(8,128)(2,1)} async-done(((bf16[256,2048]{1,0:T(8,128)(2,1)}), bf16[256,2048]{1,0:T(8,128)(2,1)}) %all-reduce.2.cloned.1.call-update) | async-done | bytes 1048592 | tf_op jit(solution)/shard_map/psum | solution.py:226
  293.9 2.0 convert_add_fusion
  295.9 56.1 %all-gather.8.cloned.1.call-done = bf16[2048,1408]{1,0:T(8,128)(2,1)} async-done(((bf16[256,1408]{1,0:T(8,128)(2,1)}), bf16[2048,1408]{1,0:T(8,128)(2,1)}) %all-gather.8.cloned.1.call-update) | async-done | bytes 5767184 | tf_op jit(solution)/shard_map/all_gather | solution.py:237
  352.0 6.3 %fusion.112 = f32[256,1408]{1,0:T(8,128)} fusion(bf16[2048,1408]{1,0:T(8,128)(2,1)} %all-gather.8.cloned.1.call-done, f32[2048]{0:T(1024)S(1)} %copy-done.33, f32[256]{0:T(256)S(1)} %add_rsqrt_fusion.2, bf16[256,2048]{1,0:T(8,128)(2,1)} %all-reduce.2.cloned.1.call-done, bf16[256,2048]{1,0:T(8,128)(2,1)} %param.27), kind=kOutput, calls=%fused_computation.189 | convolution fusion | flops 1479540736 | bytes 9315328 | tf_op jit(solution)/shard_map/dot_general | solution.py:240
  358.3 86.1 %all-gather.10.cloned.1.call-done = bf16[2048,1408]{1,0:T(8,128)(2,1)} async-done(((bf16[256,1408]{1,0:T(8,128)(2,1)}), bf16[2048,1408]{1,0:T(8,128)(2,1)}) %all-gather.10.cloned.1.call-update) | async-done | bytes 5767184 | tf_op jit(solution)/shard_map/all_gather | solution.py:238
  444.4 93.0 %all-gather.12.cloned.1.call-done = bf16[1408,2048]{1,0:T(8,128)(2,1)} async-done(((bf16[1408,256]{1,0:T(8,128)(2,1)}), bf16[1408,2048]{1,0:T(8,128)(2,1)}) %all-gather.12.cloned.1.call-update) | async-done | bytes 5767184 | tf_op jit(solution)/shard_map/all_gather | solution.py:243
  537.3 9.9 %convolution_convert_fusion = bf16[256,2048]{1,0:T(8,128)(2,1)} fusion(bf16[1408,2048]{1,0:T(8,128)(2,1)} %all-gather.12.cloned.1.call-done, bf16[2048,1408]{1,0:T(8,128)(2,1)} %all-gather.10.cloned.1.call-done, f32[256,1408]{1,0:T(8,128)} %fusion.112, f32[2048]{0:T(1024)S(1)} %copy-done.33, f32[256]{0:T(256)S(1)} %add_rsqrt_fusion.2, ...), kind=kOutput, calls=%fused_computation.60 | convolution fusion | flops 2958622720 | bytes 16131072 | tf_op jit(solution)/shard_map/dot_general | solution.py:245
  547.2 23.1 %reduce-scatter.2.cloned.1.call-done = bf16[64,2048]{1,0:T(8,128)(2,1)} async-done(((bf16[256,2048]{1,0:T(8,128)(2,1)}), bf16[64,2048]{1,0:T(8,128)(2,1)}) %reduce-scatter.2.cloned.1.call-update) | async-done | bytes 262160 | tf_op jit(solution)/shard_map/reduce_scatter | solution.py:244
  570.3 1.7 add_convert_fusion
  (260 shorter events, 44.1 us)
Async XLA Ops:
  7.4 248.9 %copy-start = (bf16[256,2048]{1,0:T(8,128)(2,1)S(1)}, bf16[256,2048]{1,0:T(8,128)(2,1)}, u32[]{:S(2)}) copy-start(bf16[256,2048]{1,0:T(8,128)(2,1)} %param.40) | copy-start | bytes 3145732
  7.4 5.3 copy-start.23
  7.4 6.3 %copy-start.3 = (bf16[256,256]{1,0:T(8,128)(2,1)S(1)}, bf16[256,256]{1,0:T(8,128)(2,1)}, u32[]{:S(2)}) copy-start(bf16[256,256]{1,0:T(8,128)(2,1)} %param.30) | copy-start | bytes 393220
  7.4 286.5 %all-reduce.2.cloned.1.call-start = ((), (), s32[]{:S(2)}) async-start(), calls=%async_computation.1 | async-start | bytes 2097152 | tf_op jit(solution)/shard_map/psum | solution.py:226
  8.4 6.9 %copy-start.18 = (bf16[256,256]{1,0:T(8,128)(2,1)S(1)}, bf16[256,256]{1,0:T(8,128)(2,1)}, u32[]{:S(2)}) copy-start(bf16[256,256]{1,0:T(8,128)(2,1)} %param.33) | copy-start | bytes 393220
  9.7 33.3 %copy-start.28 = (pred[8]{0:T(512)(128)(4,1)}, pred[8]{0:T(512)(128)(4,1)S(1)}, u32[]{:S(2)}) copy-start(pred[8]{0:T(512)(128)(4,1)S(1)} %get-tuple-element.377) | copy-start | bytes 28
  9.7 33.3 %copy-start.30 = (pred[8]{0:T(512)(128)(4,1)}, pred[8]{0:T(512)(128)(4,1)S(1)}, u32[]{:S(2)}) copy-start(pred[8]{0:T(512)(128)(4,1)S(1)} %get-tuple-element.378) | copy-start | bytes 28
  9.9 7.3 %copy-start.19 = (bf16[256,256]{1,0:T(8,128)(2,1)S(1)}, bf16[256,256]{1,0:T(8,128)(2,1)}, u32[]{:S(2)}) copy-start(bf16[256,256]{1,0:T(8,128)(2,1)} %param.34) | copy-start | bytes 393220
  12.8 32.6 %copy-start.4 = (f32[256,128]{0,1:T(8,128)}, f32[256,128]{0,1:T(8,128)S(1)}, u32[]{:S(2)}) copy-start(f32[256,128]{0,1:T(8,128)S(1)} %convert_element_type.93) | copy-start | bytes 393220
  12.8 5.6 copy-start.6
  87.6 2.2 copy-start.25
  87.6 4.4 copy-start.5
  88.2 37.0 %copy-start.12 = (f32[4,64,2,64]{1,0,3,2:T(4,128)S(1)}, f32[4,64,2,64]{1,0,3,2:T(4,128)}, u32[]{:S(2)}) copy-start(f32[4,64,2,64]{1,0,3,2:T(4,128)} %reshape_reshape.29) | copy-start | bytes 393220
  89.6 36.0 %copy-start.8 = (f32[4,64,2,64]{1,0,3,2:T(4,128)S(1)}, f32[4,64,2,64]{1,0,3,2:T(4,128)}, u32[]{:S(2)}) copy-start(f32[4,64,2,64]{1,0,3,2:T(4,128)} %reshape.253) | copy-start | bytes 393220
  89.6 36.1 %copy-start.9 = (f32[4,64,2,64]{1,0,3,2:T(4,128)S(1)}, f32[4,64,2,64]{1,0,3,2:T(4,128)}, u32[]{:S(2)}) copy-start(f32[4,64,2,64]{1,0,3,2:T(4,128)} %reshape.254) | copy-start | bytes 393220
  125.3 1.3 copy-start.11
  126.6 4.1 copy-start.16
  128.4 3.4 copy-start.20
  128.4 3.5 copy-start.27
  130.7 17.8 %copy-start.29 = (pred[8]{0:T(512)(128)(4,1)S(1)}, pred[8]{0:T(512)(128)(4,1)}, u32[]{:S(2)}) copy-start(pred[8]{0:T(512)(128)(4,1)} %copy-done.28) | copy-start | bytes 28
  130.7 17.8 %copy-start.31 = (pred[8]{0:T(512)(128)(4,1)S(1)}, pred[8]{0:T(512)(128)(4,1)}, u32[]{:S(2)}) copy-start(pred[8]{0:T(512)(128)(4,1)} %copy-done.30) | copy-start | bytes 28
  153.2 38.4 %copy-start.10 = (f32[256,256]{0,1:T(8,128)S(1)}, f32[256,256]{0,1:T(8,128)}, u32[]{:S(2)}) copy-start(f32[256,256]{0,1:T(8,128)} %convert_element_type.101) | copy-start | bytes 786436
  194.3 2.1 copy-start.17
  197.6 9.3 %copy-start.13 = (f32[4,2,64,64]{3,2,1,0:T(8,128)S(1)}, f32[4,2,64,64]{3,2,1,0:T(8,128)}, u32[]{:S(2)}) copy-start(f32[4,2,64,64]{3,2,1,0:T(8,128)} %convolution_select_fusion) | copy-start | bytes 393220
  206.9 1.6 copy-start.24
  208.3 3.4 copy-start.7
  209.8 36.8 %copy-start.1 = (f32[4,64,2,128]{1,0,3,2:T(4,128)S(1)}, f32[4,64,2,128]{1,0,3,2:T(4,128)}, u32[]{:S(2)}) copy-start(f32[4,64,2,128]{1,0,3,2:T(4,128)} %reshape.255) | copy-start | bytes 786436
  210.5 36.3 %copy-start.2 = (f32[4,64,2,128]{1,0,3,2:T(4,128)S(1)}, f32[4,64,2,128]{1,0,3,2:T(4,128)}, u32[]{:S(2)}) copy-start(f32[4,64,2,128]{1,0,3,2:T(4,128)} %reshape.256) | copy-start | bytes 786436
  246.8 2.0 copy-start.22
  251.0 2.9 copy-start.15
  253.9 1.6 copy-start.21
  253.9 1.8 copy-start.26
  253.9 1.8 copy-start.32
  256.0 1.2 copy-start.14
  258.7 93.3 %all-gather.8.cloned.1.call-start = ((), (), s32[]{:S(2)}) async-start(), calls=%async_computation.2 | async-start | bytes 6488064 | tf_op jit(solution)/shard_map/all_gather | solution.py:237
  259.3 185.1 %all-gather.10.cloned.1.call-start = ((), (), s32[]{:S(2)}) async-start(), calls=%async_computation.3 | async-start | bytes 6488064 | tf_op jit(solution)/shard_map/all_gather | solution.py:238
  259.8 277.5 %all-gather.12.cloned.1.call-start = ((), (), s32[]{:S(2)}) async-start(), calls=%async_computation.4 | async-start | bytes 6488064 | tf_op jit(solution)/shard_map/all_gather | solution.py:243
  260.4 91.6 %copy-start.33 = (f32[2048]{0:T(1024)S(1)}, f32[2048]{0:T(1024)}, u32[]{:S(2)}) copy-start(f32[2048]{0:T(1024)} %param.42) | copy-start | bytes 24580
  260.4 309.9 %reduce-scatter.2.cloned.1.call-start = ((), (), s32[]{:S(2)}) async-start(), calls=%async_computation.5 | async-start | bytes 1310720 | tf_op jit(solution)/shard_map/reduce_scatter | solution.py:244
Sparse Core Ops, SparseCore 0:
  258.8 35.0 all-reduce.1
  547.4 22.9 reduce-scatter.1
Sparse Core Ops, SparseCore 1:
  261.3 90.6 all-gather.7
  354.1 90.2 all-gather.9
  446.3 91.0 all-gather.11
where the time goes:
time: 581 us; the launch traced here: 580 us
  waiting for transfers between devices  293 us (50%)
  blocking collectives  171 us (29%)
  matrix products  50.9 us (9%)
  local copies, waits for them, and re-layouts  33.3 us (6%)
  between operations  16.2 us (3%)
  other arithmetic  14.3 us (2%)
    all_gather x1, waiting for transfers between devices, per_device(): down_whole = lax.all_gather(down_weight, 'sp', axis=1, tiled=True)  93 us
    all_gather x1, waiting for transfers between devices, per_device(): lax.all_gather(up_weight, 'sp', axis=0, tiled=True)  86.1 us
    all_gather x1, waiting for transfers between devices, per_device(): lax.all_gather(gate_weight, 'sp', axis=0, tiled=True)  56.1 us
    all_gather x1, blocking collectives, per_device(): lax.all_gather(behind_second[1][None].astype(jnp.bfloat16), 'sp', axis=0,...  33.5 us
    psum x1, waiting for transfers between devices, per_device(): lax.psum((jnp.dot(first_group_output, first_output_weight, preferred_elem...  33.2 us
    all_gather x1, blocking collectives, per_device(): lax.all_gather(ahead_second[1][None].astype(jnp.bfloat16), 'sp', axis=0,...  33.2 us
    all_gather x1, blocking collectives, per_device(): lax.all_gather(ahead_first[1][None].astype(jnp.bfloat16), 'sp', axis=0, t...  32.8 us
    all_gather x1, blocking collectives, per_device(): lax.all_gather(behind_first[1][None].astype(jnp.bfloat16), 'sp', axis=0,...  32.8 us
  transfers between devices with their start and end apart: 5, of which 5 were waited for; matrix products, arithmetic and copies ran while one was open for 1% of the time, Pallas kernels for 0%

commit v1 on v0

--- a/solution.py
+++ b/solution.py
@@ -10,6 +10,10 @@
 decay_softness = 16.0
 norm_eps = 1e-06
 highest = lax.Precision.HIGHEST
+
+
+def area_launch(in_array, chip_axis):
+    return jnp.sum(lax.all_gather(in_array, chip_axis), axis=0)
 
 
 def channel_log_decays(decay_logits, position_log_decay, key_channels):
@@ -223,7 +227,7 @@
     )
     part_rows = tok_rows // lax.axis_size("tp")
     row_start = lax.axis_index("tp") * part_rows
-    summed = lax.psum(
+    summed = area_launch(
         (
             jnp.dot(first_group_output, first_output_weight, preferred_element_type=jnp.float32)
             + jnp.dot(second_group_output, second_output_weight, preferred_element_type=jnp.float32)

time: 581 us -> 613 us (1.055)
  waiting for transfers between devices: 293 us -> 326 us
    all_gather x1, waiting for transfers between devices: 56.1 us -> 89.6 us  [per_device(): lax.all_gather(gate_weight, 'sp', axis=0, tiled=True)]
    psum x1 -> x0, waiting for transfers between devices: 33.2 us -> none  [per_device(): lax.psum((jnp.dot(first_group_output, first_output_weight, preferred_elem...]
    all_gather x0 -> x1, waiting for transfers between devices: none -> 30.8 us  [area_launch(): return jnp.sum(lax.all_gather(in_array, chip_axis), axis=0)]
  transfers between devices with their start and end apart: 5 -> 5, of which waited for: 5 -> 5; matrix products, arithmetic and copies ran while one was open for 1% -> 2% of each run, Pallas kernels for 0% -> 0%
where the time goes in v1:
time: 613 us; the launch traced here: 612 us
  waiting for transfers between devices  326 us (53%)
  blocking collectives  171 us (28%)
  matrix products  49.7 us (8%)
  local copies, waits for them, and re-layouts  33.3 us (5%)
  other arithmetic  17.3 us (3%)
  between operations  14.3 us (2%)
    all_gather x1, waiting for transfers between devices, per_device(): down_whole = lax.all_gather(down_weight, 'sp', axis=1, tiled=True)  93.2 us
    all_gather x1, waiting for transfers between devices, per_device(): lax.all_gather(gate_weight, 'sp', axis=0, tiled=True)  89.6 us
    all_gather x1, waiting for transfers between devices, per_device(): lax.all_gather(up_weight, 'sp', axis=0, tiled=True)  87.1 us
    all_gather x1, blocking collectives, per_device(): lax.all_gather(behind_second[1][None].astype(jnp.bfloat16), 'sp', axis=0,...  33.5 us
    all_gather x1, blocking collectives, per_device(): lax.all_gather(ahead_second[1][None].astype(jnp.bfloat16), 'sp', axis=0,...  33.2 us
    all_gather x1, blocking collectives, per_device(): lax.all_gather(ahead_first[1][None].astype(jnp.bfloat16), 'sp', axis=0, t...  32.8 us
    all_gather x1, blocking collectives, per_device(): lax.all_gather(behind_first[1][None].astype(jnp.bfloat16), 'sp', axis=0,...  32.8 us
    all_gather x1, waiting for transfers between devices, area_launch(): return jnp.sum(lax.all_gather(in_array, chip_axis), axis=0)  30.8 us
  transfers between devices with their start and end apart: 5, of which 5 were waited for; matrix products, arithmetic and copies ran while one was open for 2% of the time, Pallas kernels for 0%

profile of v1, /device:TPU:0, one launch (start us, length us, event | category | flops | bytes accessed | tf_op | source)
XLA Modules:
  0.0 612.3 jit_solution(18404025810015560495)
XLA Ops:
  6.6 1.0 copy.247
  10.0 0.9 copy.244
  12.0 0.9 reshape.255
  15.3 1.0 reshape.256
  16.5 1.1 reshape.257
  19.9 22.3 %all_gather.33 = f32[8,2,64]{2,1,0:T(2,128)S(1)} all-gather(f32[1,2,64]{2,1,0:T(2,128)S(1)} %broadcast_in_dim.108), channel_id=1, replica_groups=mesh['sp'=8,'tp'=4] {'sp'}, dimensions={0}, use_global_device_ids=true | all-gather | bytes 4608 | tf_op jit(solution)/shard_map/all_gather | solution.py:148
  43.0 1.2 reduce-window.30
  45.9 32.8 %all-gather.1 = bf16[16,64,128]{2,1,0:T(8,128)(2,1)} all-gather(bf16[2,64,128]{2,1,0:T(8,128)(2,1)S(1)} %convolution_convert_fusion.4), channel_id=3, replica_groups=mesh['sp'=8,'tp'=4] {'sp'}, dimensions={0}, use_global_device_ids=true | all-gather | bytes 294912 | tf_op jit(solution)/shard_map/all_gather | solution.py:175
  79.8 1.6 fusion.71
  82.2 4.6 while.49
  87.4 1.4 fusion.44
  89.7 1.2 reduce-window.26
  91.5 32.8 %all-gather = bf16[16,64,128]{2,1,0:T(8,128)(2,1)} all-gather(bf16[2,64,128]{2,1,0:T(8,128)(2,1)S(1)} %convolution_convert_fusion.3), channel_id=2, replica_groups=mesh['sp'=8,'tp'=4] {'sp'}, dimensions={0}, use_global_device_ids=true | all-gather | bytes 294912 | tf_op jit(solution)/shard_map/all_gather | solution.py:172
  125.9 1.6 fusion.73
  127.6 2.3 while.48
  131.3 16.3 %all_gather.36 = f32[8,2,128]{2,1,0:T(2,128)S(1)} all-gather(f32[1,2,128]{2,1,0:T(2,128)S(1)} %bitcast.426), channel_id=1, replica_groups=mesh['sp'=8,'tp'=4] {'sp'}, dimensions={0}, use_global_device_ids=true | all-gather | bytes 9216 | tf_op jit(solution)/shard_map/all_gather | solution.py:149
  152.4 2.0 rev.40
  154.7 1.4 convolution_convert_fusion.1
  156.1 33.5 %all-gather.3 = bf16[16,128,128]{2,1,0:T(8,128)(2,1)} all-gather(bf16[2,128,128]{2,1,0:T(8,128)(2,1)S(1)} %convolution_convert_fusion.1), channel_id=5, replica_groups=mesh['sp'=8,'tp'=4] {'sp'}, dimensions={0}, use_global_device_ids=true | all-gather | bytes 589824 | tf_op jit(solution)/shard_map/all_gather | solution.py:181
  189.6 1.0 copy.305
  190.9 1.6 rev.37
  192.4 1.1 copy.302
  193.5 1.3 convolution_select_fusion
  195.6 1.2 fusion.46
  197.5 8.6 %while.51 = (s32[]{:T(128)}, f32[2,128,128]{2,1,0:T(8,128)S(1)}, f32[4,2,64,128]{3,2,1,0:T(8,128)}, f32[4,2,1,128]{3,1,2,0:T(2,128)S(1)}, f32[4,2,64,128]{3,2,1,...) while((s32[]{:T(128)}, f32[2,128,128]{2,1,0:T(8,128)S(1)}, ...), condition=%wide.region_26.27_spmd, body=%wide.region_25.26_spmd.sunk | while | flops 50397184 | bytes 660569 | solution.py:58
  198.4 1.2 convolution_add_fusion.16
  200.5 1.2 convolution_add_fusion.16
  202.7 1.2 convolution_add_fusion.16
  204.8 1.2 convolution_add_fusion.16
  206.1 1.3 fusion.42
  209.7 1.1 copy.295
  211.1 33.2 %all-gather.2 = bf16[16,128,128]{2,1,0:T(8,128)(2,1)} all-gather(bf16[2,128,128]{2,1,0:T(8,128)(2,1)S(1)} %convolution_convert_fusion.2), channel_id=4, replica_groups=mesh['sp'=8,'tp'=4] {'sp'}, dimensions={0}, use_global_device_ids=true | all-gather | bytes 589824 | tf_op jit(solution)/shard_map/all_gather | solution.py:178
  244.3 1.1 reshape_reshape.34
  246.8 1.1 reshape_reshape.37
  247.9 2.2 fusion.48
  250.2 2.9 while.50
  253.5 1.0 copy.278
  256.4 1.5 fusion.41
  260.2 30.8 %all-gather.16.cloned.1.call-done = bf16[1024,2048]{1,0:T(8,128)(2,1)} async-done(((bf16[256,2048]{1,0:T(8,128)(2,1)}), bf16[1024,2048]{1,0:T(8,128)(2,1)}) %all-gather.16.cloned.1.call-update) | async-done | bytes 4194320 | tf_op jit(solution)/shard_map/all_gather | solution.py:16
  291.0 3.2 reduce_sum.81
  294.2 1.7 convert_add_fusion
  295.9 89.6 %all-gather.10.cloned.1.call-done = bf16[2048,1408]{1,0:T(8,128)(2,1)} async-done(((bf16[256,1408]{1,0:T(8,128)(2,1)}), bf16[2048,1408]{1,0:T(8,128)(2,1)}) %all-gather.10.cloned.1.call-update) | async-done | bytes 5767184 | tf_op jit(solution)/shard_map/all_gather | solution.py:241
  385.5 5.6 fusion.112
  391.1 87.1 %all-gather.12.cloned.1.call-done = bf16[2048,1408]{1,0:T(8,128)(2,1)} async-done(((bf16[256,1408]{1,0:T(8,128)(2,1)}), bf16[2048,1408]{1,0:T(8,128)(2,1)}) %all-gather.12.cloned.1.call-update) | async-done | bytes 5767184 | tf_op jit(solution)/shard_map/all_gather | solution.py:242
  478.2 93.2 %all-gather.14.cloned.1.call-done = bf16[1408,2048]{1,0:T(8,128)(2,1)} async-done(((bf16[1408,256]{1,0:T(8,128)(2,1)}), bf16[1408,2048]{1,0:T(8,128)(2,1)}) %all-gather.14.cloned.1.call-update) | async-done | bytes 5767184 | tf_op jit(solution)/shard_map/all_gather | solution.py:247
  571.5 9.2 %convolution_convert_fusion = bf16[256,2048]{1,0:T(8,128)(2,1)} fusion(bf16[1408,2048]{1,0:T(8,128)(2,1)} %all-gather.14.cloned.1.call-done, bf16[2048,1408]{1,0:T(8,128)(2,1)} %all-gather.12.cloned.1.call-done, f32[256,1408]{1,0:T(8,128)} %fusion.112, f32[2048]{0:T(1024)S(1)} %copy-done.34, f32[256]{0:T(256)S(1)} %add_rsqrt_fusion.2, ...), kind=kOutput, calls=%fused_computation.60 | convolution fusion | flops 2958622720 | bytes 16131072 | tf_op jit(solution)/shard_map/dot_general | solution.py:249
  580.7 23.1 %reduce-scatter.2.cloned.1.call-done = bf16[64,2048]{1,0:T(8,128)(2,1)} async-done(((bf16[256,2048]{1,0:T(8,128)(2,1)}), bf16[64,2048]{1,0:T(8,128)(2,1)}) %reduce-scatter.2.cloned.1.call-update) | async-done | bytes 262160 | tf_op jit(solution)/shard_map/reduce_scatter | solution.py:248
  603.9 1.9 add_convert_fusion
  (263 shorter events, 45.3 us)
Async XLA Ops:
  6.5 248.9 %copy-start = (bf16[256,2048]{1,0:T(8,128)(2,1)S(1)}, bf16[256,2048]{1,0:T(8,128)(2,1)}, u32[]{:S(2)}) copy-start(bf16[256,2048]{1,0:T(8,128)(2,1)} %param.40) | copy-start | bytes 3145732
  6.5 5.3 copy-start.24
  6.5 6.3 %copy-start.3 = (bf16[256,256]{1,0:T(8,128)(2,1)S(1)}, bf16[256,256]{1,0:T(8,128)(2,1)}, u32[]{:S(2)}) copy-start(bf16[256,256]{1,0:T(8,128)(2,1)} %param.30) | copy-start | bytes 393220
  6.5 284.4 %all-gather.16.cloned.1.call-start = ((), (), s32[]{:S(2)}) async-start(), calls=%async_computation.5 | async-start | bytes 5242880 | tf_op jit(solution)/shard_map/all_gather | solution.py:16
  7.6 6.9 %copy-start.19 = (bf16[256,256]{1,0:T(8,128)(2,1)S(1)}, bf16[256,256]{1,0:T(8,128)(2,1)}, u32[]{:S(2)}) copy-start(bf16[256,256]{1,0:T(8,128)(2,1)} %param.33) | copy-start | bytes 393220
  8.9 33.3 %copy-start.29 = (pred[8]{0:T(512)(128)(4,1)}, pred[8]{0:T(512)(128)(4,1)S(1)}, u32[]{:S(2)}) copy-start(pred[8]{0:T(512)(128)(4,1)S(1)} %get-tuple-element.377) | copy-start | bytes 28
  8.9 33.3 %copy-start.31 = (pred[8]{0:T(512)(128)(4,1)}, pred[8]{0:T(512)(128)(4,1)S(1)}, u32[]{:S(2)}) copy-start(pred[8]{0:T(512)(128)(4,1)S(1)} %get-tuple-element.378) | copy-start | bytes 28
  9.1 7.3 %copy-start.20 = (bf16[256,256]{1,0:T(8,128)(2,1)S(1)}, bf16[256,256]{1,0:T(8,128)(2,1)}, u32[]{:S(2)}) copy-start(bf16[256,256]{1,0:T(8,128)(2,1)} %param.34) | copy-start | bytes 393220
  11.9 32.6 %copy-start.4 = (f32[256,128]{0,1:T(8,128)}, f32[256,128]{0,1:T(8,128)S(1)}, u32[]{:S(2)}) copy-start(f32[256,128]{0,1:T(8,128)S(1)} %convert_element_type.95) | copy-start | bytes 393220
  12.0 5.6 copy-start.6
  86.7 2.2 copy-start.26
  86.8 4.4 copy-start.5
  87.4 37.0 %copy-start.13 = (f32[4,64,2,64]{1,0,3,2:T(4,128)S(1)}, f32[4,64,2,64]{1,0,3,2:T(4,128)}, u32[]{:S(2)}) copy-start(f32[4,64,2,64]{1,0,3,2:T(4,128)} %reshape_reshape.29) | copy-start | bytes 393220
  88.8 36.0 %copy-start.9 = (f32[4,64,2,64]{1,0,3,2:T(4,128)S(1)}, f32[4,64,2,64]{1,0,3,2:T(4,128)}, u32[]{:S(2)}) copy-start(f32[4,64,2,64]{1,0,3,2:T(4,128)} %reshape.254) | copy-start | bytes 393220
  88.8 36.1 %copy-start.10 = (f32[4,64,2,64]{1,0,3,2:T(4,128)S(1)}, f32[4,64,2,64]{1,0,3,2:T(4,128)}, u32[]{:S(2)}) copy-start(f32[4,64,2,64]{1,0,3,2:T(4,128)} %reshape.255) | copy-start | bytes 393220
  124.5 1.3 copy-start.12
  125.8 4.1 copy-start.17
  127.6 3.4 copy-start.21
  127.6 3.5 copy-start.28
  129.9 17.8 %copy-start.30 = (pred[8]{0:T(512)(128)(4,1)S(1)}, pred[8]{0:T(512)(128)(4,1)}, u32[]{:S(2)}) copy-start(pred[8]{0:T(512)(128)(4,1)} %copy-done.29) | copy-start | bytes 28
  129.9 17.8 %copy-start.32 = (pred[8]{0:T(512)(128)(4,1)S(1)}, pred[8]{0:T(512)(128)(4,1)}, u32[]{:S(2)}) copy-start(pred[8]{0:T(512)(128)(4,1)} %copy-done.31) | copy-start | bytes 28
  152.4 38.4 %copy-start.11 = (f32[256,256]{0,1:T(8,128)S(1)}, f32[256,256]{0,1:T(8,128)}, u32[]{:S(2)}) copy-start(f32[256,256]{0,1:T(8,128)} %convert_element_type.103) | copy-start | bytes 786436
  193.5 2.1 copy-start.18
  196.8 9.3 %copy-start.14 = (f32[4,2,64,64]{3,2,1,0:T(8,128)S(1)}, f32[4,2,64,64]{3,2,1,0:T(8,128)}, u32[]{:S(2)}) copy-start(f32[4,2,64,64]{3,2,1,0:T(8,128)} %convolution_select_fusion) | copy-start | bytes 393220
  206.1 1.6 copy-start.25
  207.4 3.4 copy-start.7
  208.9 36.8 %copy-start.1 = (f32[4,64,2,128]{1,0,3,2:T(4,128)S(1)}, f32[4,64,2,128]{1,0,3,2:T(4,128)}, u32[]{:S(2)}) copy-start(f32[4,64,2,128]{1,0,3,2:T(4,128)} %reshape.256) | copy-start | bytes 786436
  209.7 36.3 %copy-start.2 = (f32[4,64,2,128]{1,0,3,2:T(4,128)S(1)}, f32[4,64,2,128]{1,0,3,2:T(4,128)}, u32[]{:S(2)}) copy-start(f32[4,64,2,128]{1,0,3,2:T(4,128)} %reshape.257) | copy-start | bytes 786436
  245.9 2.0 copy-start.23
  250.1 2.9 copy-start.16
  253.0 1.6 copy-start.22
  253.0 1.8 copy-start.27
  253.1 1.8 copy-start.33
  255.1 1.2 copy-start.15
  257.9 127.6 %all-gather.10.cloned.1.call-start = ((), (), s32[]{:S(2)}) async-start(), calls=%async_computation.1 | async-start | bytes 6488064 | tf_op jit(solution)/shard_map/all_gather | solution.py:241
  258.6 219.6 %all-gather.12.cloned.1.call-start = ((), (), s32[]{:S(2)}) async-start(), calls=%async_computation.2 | async-start | bytes 6488064 | tf_op jit(solution)/shard_map/all_gather | solution.py:242
  259.4 312.1 %all-gather.14.cloned.1.call-start = ((), (), s32[]{:S(2)}) async-start(), calls=%async_computation.3 | async-start | bytes 6488064 | tf_op jit(solution)/shard_map/all_gather | solution.py:247
  259.9 343.9 %reduce-scatter.2.cloned.1.call-start = ((), (), s32[]{:S(2)}) async-start(), calls=%async_computation.4 | async-start | bytes 1310720 | tf_op jit(solution)/shard_map/reduce_scatter | solution.py:248
  291.0 3.2 copy-start.8
  294.2 91.4 %copy-start.34 = (f32[2048]{0:T(1024)S(1)}, f32[2048]{0:T(1024)}, u32[]{:S(2)}) copy-start(f32[2048]{0:T(1024)} %param.42) | copy-start | bytes 24580
Sparse Core Ops, SparseCore 0:
  258.0 32.9 all-gather.15
  293.2 92.3 all-gather.9
  387.7 90.4 all-gather.11
  480.1 91.2 all-gather.13
  580.8 22.9 reduce-scatter.1
